TPU v7x, 32 devices: a whole 2x2x4 slice. The times are simulated.
32 devices in a mesh: grp: 2 (over y), ra: 4 (over z), cb: 4 (over x, core).
Axes of the slice: x: 2, y: 2, z: 4, core: 2. Of those that a mesh axis runs over, the one named last changes fastest.
Arguments:
- tokens: bfloat16 [512, 4096], P('grp', 'cb'), parts along dimension 0, may hold values from -50 to 50
- norm_gains: float32 [3, 4096], P(None, 'cb'), may hold values from 0.1 to 1.9
- gate_weight: float32 [2, 4096, 11264], P(None, 'cb', 'ra'), may hold values from -0.09375 to 0.09375
- value_weight: float32 [2, 4096, 11264], P(None, 'cb', 'ra'), may hold values from -0.09375 to 0.09375
- gate_scale: float32 [2, 11264], P(None, 'ra'), may hold values from 0.3 to 3
- value_scale: float32 [2, 11264], P(None, 'ra'), may hold values from 0.3 to 3
- conv_gate: float32 [2, 3, 11264], P(None, None, 'ra'), may hold values from -3 to 3
- conv_value: float32 [2, 3, 11264], P(None, None, 'ra'), may hold values from -3 to 3
- down_weight: float32 [2, 11264, 4096], P(None, 'ra', 'cb'), may hold values from -0.07537784 to 0.07537784
- down_scale: float32 [2, 4096], P(None, 'cb'), may hold values from 0.3 to 3
Outputs:
- normed_out: bfloat16 [512, 4096], P('grp', 'cb'), parts along dimension 0
There are 2 independent parts, one for each index of `grp`. A program takes and returns all parts, laid end to end along the dimension named above; an argument that names none is the same for every part. Nothing has to cross between parts.
All inputs are finite; a program needn't handle non-finite values.
Results may differ from a plain program's by a relative error of at most 0.012.
The roundings to bfloat16 on the way count: a program that leaves them out, or rounds other values in their place, can miss the bound.
Values may be sent and summed in bfloat16 or wider, within the bound.
A program may use at most 192 MiB of HBM per device.

v0:
```python
import jax
import jax.numpy as jnp
from jax import lax
from jax.sharding import PartitionSpec as P

epsilon = 1e-06
residual_weight = 0.5


def causal_taps(projected, tap_weights):
    tap_count = tap_weights.shape[0]
    row_count = projected.shape[0]
    padded = jnp.pad(projected, ((tap_count - 1, 0), (0, 0)))
    result = jnp.zeros_like(projected)
    for tap_idx in range(tap_count):
        result = result + padded[tap_idx : tap_idx + row_count] * tap_weights[tap_idx]
    return result


def row_inverse(state_wide, model_width):
    squares = lax.psum(jnp.sum(state_wide * state_wide, axis=1, keepdims=True), "cb")
    return lax.rsqrt(squares / model_width + epsilon)


def on_device(
    tokens,
    norm_gains,
    gate_weight,
    value_weight,
    gate_scale,
    value_scale,
    conv_gate,
    conv_value,
    down_weight,
    down_scale,
):
    model_width = lax.axis_size("cb") * tokens.shape[1]
    layer_count = gate_weight.shape[0]
    current = tokens
    for layer_idx in range(layer_count):
        state_wide = current.astype(jnp.float32)
        inverse = row_inverse(state_wide, model_width)
        scaled = (state_wide * norm_gains[layer_idx]).astype(jnp.bfloat16)
        gate_part = jnp.dot(
            scaled, gate_weight[layer_idx].astype(jnp.bfloat16), preferred_element_type=jnp.float32
        )
        value_part = jnp.dot(
            scaled, value_weight[layer_idx].astype(jnp.bfloat16), preferred_element_type=jnp.float32
        )
        gate_sum, value_sum = (
            lax.psum_scatter(gate_part, "cb", scatter_dimension=1, tiled=True),
            lax.psum_scatter(value_part, "cb", scatter_dimension=1, tiled=True),
        )
        share_cols = gate_sum.shape[1]
        first_col = lax.axis_index("cb") * share_cols
        gate_cols = lax.dynamic_slice_in_dim(gate_scale[layer_idx], first_col, share_cols, 0)
        value_cols = lax.dynamic_slice_in_dim(value_scale[layer_idx], first_col, share_cols, 0)
        gate_taps = lax.dynamic_slice_in_dim(conv_gate[layer_idx], first_col, share_cols, 1)
        value_taps = lax.dynamic_slice_in_dim(conv_value[layer_idx], first_col, share_cols, 1)
        gate_pre = inverse * gate_cols * gate_sum
        value_pre = inverse * value_cols * value_sum
        hidden = (
            jax.nn.gelu(causal_taps(gate_pre, gate_taps), approximate=True)
            * causal_taps(value_pre, value_taps)
        ).astype(jnp.bfloat16)
        hidden = lax.all_gather(hidden, "cb", axis=1, tiled=True)
        partial_value = jnp.dot(
            hidden, down_weight[layer_idx].astype(jnp.bfloat16), preferred_element_type=jnp.float32
        )
        down_total = lax.psum(partial_value, "ra")
        current = (residual_weight * state_wide + down_scale[layer_idx] * down_total).astype(
            jnp.bfloat16
        )
    state_wide = current.astype(jnp.float32)
    inverse = row_inverse(state_wide, model_width)
    return (state_wide * inverse * norm_gains[layer_count]).astype(jnp.bfloat16)


def solution(mesh):
    in_specs = (
        P("grp", "cb"),
        P(None, "cb"),
        P(None, "cb", "ra"),
        P(None, "cb", "ra"),
        P(None, "ra"),
        P(None, "ra"),
        P(None, None, "ra"),
        P(None, None, "ra"),
        P(None, "ra", "cb"),
        P(None, "cb"),
    )
    out_specs = P("grp", "cb")
    return jax.shard_map(
        on_device, mesh=mesh, in_specs=in_specs, out_specs=out_specs, check_vma=False
    )
```

profile of v0, /device:TPU:0, one launch (start us, length us, event | category | flops | bytes accessed | tf_op | source)
XLA Modules:
  0.0 362.3 jit_solution(13226815253919093914)
XLA Ops:
  7.4 8.6 %convert.12 = bf16[2,1024,2816]{2,1,0:T(8,128)(2,1)S(1)} convert(f32[2,1024,2816]{2,1,0:T(8,128)} %param.12) | non-fusion elementwise | flops 5767168 | bytes 34603008 | tf_op jit(solution)/shard_map/convert.5
  16.0 4.2 %copy-done.1 = bf16[2,1024,2816]{2,1,0:T(8,128)(2,1)} copy-done((bf16[2,1024,2816]{2,1,0:T(8,128)(2,1)}, bf16[2,1024,2816]{2,1,0:T(8,128)(2,1)S(1)}, u32[]{:S(2)}) %copy-start.1) | copy-done | bytes 11534360
  20.2 4.1 %fusion.5 = f32[256,2816]{0,1:T(8,128)} fusion(bf16[2,1024,2816]{2,1,0:T(8,128)(2,1)S(1)} %convert.12, bf16[256,1024]{1,0:T(8,128)(2,1)S(1)} %copy-done.2, f32[1024]{0:T(1024)S(1)} %bitcast.42), kind=kOutput, calls=%fused_computation.11 | convolution fusion | flops 1477181440 | bytes 9179136 | tf_op jit(solution)/shard_map/dot_general | solution.py:44
  24.4 8.6 %convert.13 = bf16[2,1024,2816]{2,1,0:T(8,128)(2,1)S(1)} convert(f32[2,1024,2816]{2,1,0:T(8,128)} %param.13) | non-fusion elementwise | flops 5767168 | bytes 34603008 | tf_op jit(solution)/shard_map/convert.4
  32.9 4.8 %copy-done = bf16[2,1024,2816]{2,1,0:T(8,128)(2,1)} copy-done((bf16[2,1024,2816]{2,1,0:T(8,128)(2,1)}, bf16[2,1024,2816]{2,1,0:T(8,128)(2,1)S(1)}, u32[]{:S(2)}) %copy-start) | copy-done | bytes 11534360
  37.8 4.0 %fusion.4 = f32[256,2816]{0,1:T(8,128)} fusion(bf16[2,1024,2816]{2,1,0:T(8,128)(2,1)S(1)} %convert.13, bf16[256,1024]{1,0:T(8,128)(2,1)S(1)} %copy-done.2, f32[1024]{0:T(1024)S(1)} %bitcast.43), kind=kOutput, calls=%fused_computation.9 | convolution fusion | flops 1477181440 | bytes 9179136 | tf_op jit(solution)/shard_map/dot_general | solution.py:47
  42.2 9.0 %psum.35 = f32[256,1]{0,1:T(1,128)S(1)} all-reduce(f32[256,1]{0,1:T(1,128)S(1)} %bitcast.39), channel_id=1, replica_groups=mesh['grp'=2,'ra'=4,'cb'=4] {'cb'}, use_global_device_ids=true, to_apply=%region_1.0 | all-reduce | flops 256 | bytes 2048 | tf_op jit(solution)/shard_map/psum | solution.py:21
  51.5 12.1 %reduce-scatter.5.cloned.1.call-done = f32[256,704]{0,1:T(8,128)} async-done(((f32[256,2816]{0,1:T(8,128)}), f32[256,704]{0,1:T(8,128)}) %reduce-scatter.5.cloned.1.call-update) | async-done | bytes 720912 | tf_op jit(solution)/shard_map/reduce_scatter | solution.py:51
  63.5 38.8 %reduce-scatter.7.cloned.1.call-done = f32[256,704]{0,1:T(8,128)} async-done(((f32[256,2816]{0,1:T(8,128)}), f32[256,704]{0,1:T(8,128)}) %reduce-scatter.7.cloned.1.call-update) | async-done | bytes 720912 | tf_op jit(solution)/shard_map/reduce_scatter | solution.py:52
  103.9 2.2 fusion.25
  106.2 12.6 %convert.14 = bf16[2,2816,1024]{2,1,0:T(8,128)(2,1)} convert(f32[2,2816,1024]{2,1,0:T(8,128)} %param.18) | non-fusion elementwise | flops 5767168 | bytes 34603008 | tf_op jit(solution)/shard_map/convert.3
  118.8 6.4 %all-gather.3.cloned.1.call-done = bf16[256,2816]{0,1:T(8,128)(2,1)} async-done(((bf16[256,704]{0,1:T(8,128)(2,1)}), bf16[256,2816]{0,1:T(8,128)(2,1)}) %all-gather.3.cloned.1.call-update) | async-done | bytes 1441808 | tf_op jit(solution)/shard_map/all_gather | solution.py:66
  125.2 5.8 %fusion.3 = f32[256,1024]{1,0:T(8,128)} fusion(bf16[256,2816]{0,1:T(8,128)(2,1)} %all-gather.3.cloned.1.call-done, bf16[2,2816,1024]{2,1,0:T(8,128)(2,1)} %convert.14), kind=kOutput, calls=%fused_computation.7 | convolution fusion | flops 1476395008 | bytes 8257536 | tf_op jit(solution)/shard_map/dot_general | solution.py:67
  131.0 52.0 %all-reduce.7.cloned.1.call-done = f32[256,1024]{1,0:T(8,128)} async-done(((f32[256,1024]{1,0:T(8,128)}), f32[256,1024]{1,0:T(8,128)}) %all-reduce.7.cloned.1.call-update) | async-done | bytes 1048592 | tf_op jit(solution)/shard_map/psum | solution.py:70
  184.5 6.6 %fusion.2 = f32[256,2816]{0,1:T(8,128)} fusion(bf16[2,1024,2816]{2,1,0:T(8,128)(2,1)} %copy-done.1, bf16[256,1024]{1,0:T(8,128)(2,1)S(1)} %get-tuple-element.20, f32[1024]{0:T(1024)S(1)} %bitcast.40), kind=kOutput, calls=%fused_computation.5 | convolution fusion | flops 1477181440 | bytes 9179136 | tf_op jit(solution)/shard_map/dot_general | solution.py:44
  191.4 6.6 %fusion.1 = f32[256,2816]{0,1:T(8,128)} fusion(bf16[2,1024,2816]{2,1,0:T(8,128)(2,1)} %copy-done, bf16[256,1024]{1,0:T(8,128)(2,1)S(1)} %get-tuple-element.20, f32[1024]{0:T(1024)S(1)} %bitcast.41), kind=kOutput, calls=%fused_computation.3 | convolution fusion | flops 1477181440 | bytes 9179136 | tf_op jit(solution)/shard_map/dot_general | solution.py:47
  198.3 6.8 %psum.37 = f32[256,1]{0,1:T(1,128)S(1)} all-reduce(f32[256,1]{0,1:T(1,128)S(1)} %bitcast.34), channel_id=1, replica_groups=mesh['grp'=2,'ra'=4,'cb'=4] {'cb'}, use_global_device_ids=true, to_apply=%region_6.7 | all-reduce | flops 256 | bytes 2048 | tf_op jit(solution)/shard_map/psum | solution.py:21
  205.2 21.6 %reduce-scatter.9.cloned.1.call-done = f32[256,704]{0,1:T(8,128)} async-done(((f32[256,2816]{0,1:T(8,128)}), f32[256,704]{0,1:T(8,128)}) %reduce-scatter.9.cloned.1.call-update) | async-done | bytes 720912 | tf_op jit(solution)/shard_map/reduce_scatter | solution.py:51
  226.8 38.6 %reduce-scatter.11.cloned.1.call-done = f32[256,704]{0,1:T(8,128)} async-done(((f32[256,2816]{0,1:T(8,128)}), f32[256,704]{0,1:T(8,128)}) %reduce-scatter.11.cloned.1.call-update) | async-done | bytes 720912 | tf_op jit(solution)/shard_map/reduce_scatter | solution.py:52
  267.0 2.2 fusion.34
  269.3 19.0 %all-gather.5.cloned.1.call-done = bf16[256,2816]{0,1:T(8,128)(2,1)} async-done(((bf16[256,704]{0,1:T(8,128)(2,1)}), bf16[256,2816]{0,1:T(8,128)(2,1)}) %all-gather.5.cloned.1.call-update) | async-done | bytes 1441808 | tf_op jit(solution)/shard_map/all_gather | solution.py:66
  288.3 5.7 %fusion = f32[256,1024]{1,0:T(8,128)} fusion(bf16[256,2816]{0,1:T(8,128)(2,1)} %all-gather.5.cloned.1.call-done, bf16[2,2816,1024]{2,1,0:T(8,128)(2,1)} %convert.14), kind=kOutput, calls=%fused_computation.1 | convolution fusion | flops 1476395008 | bytes 8257536 | tf_op jit(solution)/shard_map/dot_general | solution.py:67
  294.0 52.1 %all-reduce.9.cloned.1.call-done = f32[256,1024]{1,0:T(8,128)} async-done(((f32[256,1024]{1,0:T(8,128)}), f32[256,1024]{1,0:T(8,128)}) %all-reduce.9.cloned.1.call-update) | async-done | bytes 1048592 | tf_op jit(solution)/shard_map/psum | solution.py:70
  347.6 6.8 %psum.39 = f32[256,1]{0,1:T(1,128)S(1)} all-reduce(f32[256,1]{0,1:T(1,128)S(1)} %bitcast.37), channel_id=1, replica_groups=mesh['grp'=2,'ra'=4,'cb'=4] {'cb'}, use_global_device_ids=true, to_apply=%region_11.12 | all-reduce | flops 256 | bytes 2048 | tf_op jit(solution)/shard_map/psum | solution.py:21
  (49 shorter events, 9.5 us)
Async XLA Ops:
  6.5 57.0 %reduce-scatter.5.cloned.1.call-start = ((), (), s32[]{:S(2)}) async-start(), calls=%async_computation.4 | async-start | bytes 3604480 | tf_op jit(solution)/shard_map/reduce_scatter | solution.py:51
  7.4 12.8 %copy-start.2 = (bf16[256,1024]{1,0:T(8,128)(2,1)S(1)}, bf16[256,1024]{1,0:T(8,128)(2,1)}, u32[]{:S(2)}) copy-start(bf16[256,1024]{1,0:T(8,128)(2,1)} %param.10) | copy-start | bytes 1572868
  16.0 4.2 %copy-start.1 = (bf16[2,1024,2816]{2,1,0:T(8,128)(2,1)}, bf16[2,1024,2816]{2,1,0:T(8,128)(2,1)S(1)}, u32[]{:S(2)}) copy-start(bf16[2,1024,2816]{2,1,0:T(8,128)(2,1)S(1)} %convert.12) | copy-start | bytes 34603012
  24.3 78.0 %reduce-scatter.7.cloned.1.call-start = ((), (), s32[]{:S(2)}) async-start(), calls=%async_computation.5 | async-start | bytes 3604480 | tf_op jit(solution)/shard_map/reduce_scatter | solution.py:52
  32.9 4.8 %copy-start = (bf16[2,1024,2816]{2,1,0:T(8,128)(2,1)}, bf16[2,1024,2816]{2,1,0:T(8,128)(2,1)S(1)}, u32[]{:S(2)}) copy-start(bf16[2,1024,2816]{2,1,0:T(8,128)(2,1)S(1)} %convert.13) | copy-start | bytes 34603012
  37.7 4.1 %copy-start.5 = (f32[2,2816]{1,0:T(2,128)S(1)}, f32[2,2816]{1,0:T(2,128)}, u32[]{:S(2)}) copy-start(f32[2,2816]{1,0:T(2,128)} %param.14) | copy-start | bytes 67588
  37.7 4.1 %copy-start.6 = (f32[2,2816]{1,0:T(2,128)S(1)}, f32[2,2816]{1,0:T(2,128)}, u32[]{:S(2)}) copy-start(f32[2,2816]{1,0:T(2,128)} %param.15) | copy-start | bytes 67588
  37.8 13.5 %copy-start.3 = (f32[2,3,2816]{2,0,1:T(2,128)S(1)}, f32[2,3,2816]{2,0,1:T(2,128)}, u32[]{:S(2)}) copy-start(f32[2,3,2816]{2,0,1:T(2,128)} %param.16) | copy-start | bytes 202756
  37.8 13.5 %copy-start.4 = (f32[2,3,2816]{2,0,1:T(2,128)S(1)}, f32[2,3,2816]{2,0,1:T(2,128)}, u32[]{:S(2)}) copy-start(f32[2,3,2816]{2,0,1:T(2,128)} %param.17) | copy-start | bytes 202756
  41.8 83.4 %all-gather.3.cloned.1.call-start = ((), (), s32[]{:S(2)}) async-start(), calls=%async_computation.6 | async-start | bytes 1802240 | tf_op jit(solution)/shard_map/all_gather | solution.py:66
  106.1 76.9 %all-reduce.7.cloned.1.call-start = ((), (), s32[]{:S(2)}) async-start(), calls=%async_computation.7 | async-start | bytes 2097152 | tf_op jit(solution)/shard_map/psum | solution.py:70
  118.8 12.2 %copy-start.7 = (f32[2,1024]{1,0:T(2,128)S(1)}, f32[2,1024]{1,0:T(2,128)}, u32[]{:S(2)}) copy-start(f32[2,1024]{1,0:T(2,128)} %param.19) | copy-start | bytes 24580
  130.9 95.8 %reduce-scatter.9.cloned.1.call-start = ((), (), s32[]{:S(2)}) async-start(), calls=%async_computation.8 | async-start | bytes 3604480 | tf_op jit(solution)/shard_map/reduce_scatter | solution.py:51
  191.2 74.2 %reduce-scatter.11.cloned.1.call-start = ((), (), s32[]{:S(2)}) async-start(), calls=%async_computation.9 | async-start | bytes 3604480 | tf_op jit(solution)/shard_map/reduce_scatter | solution.py:52
  198.1 90.2 %all-gather.5.cloned.1.call-start = ((), (), s32[]{:S(2)}) async-start(), calls=%async_computation.10 | async-start | bytes 1802240 | tf_op jit(solution)/shard_map/all_gather | solution.py:66
  269.2 76.9 %all-reduce.9.cloned.1.call-start = ((), (), s32[]{:S(2)}) async-start(), calls=%async_computation.11 | async-start | bytes 2097152 | tf_op jit(solution)/shard_map/psum | solution.py:70
Sparse Core Ops, SparseCore 0:
  24.4 39.0 reduce-scatter.4
  66.1 36.1 reduce-scatter.6
  106.2 18.8 all-gather.2
  131.1 51.8 all-reduce.6
  191.3 35.4 reduce-scatter.8
  229.2 36.1 reduce-scatter.10
  269.3 18.8 all-gather.4
  294.1 51.8 all-reduce.8
where the time goes:
time: 363 us; the launch traced here: 362 us
  waiting for transfers between devices  241 us (66%)
  other arithmetic  41.6 us (11%)
  matrix products  32.8 us (9%)
  blocking collectives  22.7 us (6%)
  between operations  13.7 us (4%)
  local copies, waits for them, and re-layouts  10.5 us (3%)
    psum x2, waiting for transfers between devices, on_device(): down_total = lax.psum(partial_value, 'ra')  104 us
    reduce_scatter x2, waiting for transfers between devices, on_device(): lax.psum_scatter(value_part, 'cb', scatter_dimension=1, tiled=True)  77.4 us
    reduce_scatter x2, waiting for transfers between devices, on_device(): lax.psum_scatter(gate_part, 'cb', scatter_dimension=1, tiled=True)  33.6 us
    another operation x3, other arithmetic  29.8 us
    all_gather x2, waiting for transfers between devices, on_device(): hidden = lax.all_gather(hidden, 'cb', axis=1, tiled=True)  25.4 us
    psum x3, blocking collectives, row_inverse(): lax.psum(jnp.sum(state_wide * state_wide, axis=1, keepdims=True), 'cb')  22.7 us
    dot_general x2, matrix products, on_device(): jnp.dot(hidden, down_weight[layer_idx].astype(jnp.bfloat16), preferred_el...  11.5 us
    dot_general x2, matrix products, on_device(): jnp.dot(scaled, gate_weight[layer_idx].astype(jnp.bfloat16), preferred_el...  10.7 us
  transfers between devices with their start and end apart: 8, of which 8 were waited for; matrix products, arithmetic and copies ran while one was open for 9% of the time, Pallas kernels for 0%

commit v1 on v0

--- a/solution.py
+++ b/solution.py
@@ -67,7 +67,11 @@
         partial_value = jnp.dot(
             hidden, down_weight[layer_idx].astype(jnp.bfloat16), preferred_element_type=jnp.float32
         )
-        down_total = lax.psum(partial_value, "ra")
+        down_total = partial_value
+        for hop in (1, 2):
+            down_total = down_total + lax.ppermute(
+                down_total, "ra", [(dev, dev ^ hop) for dev in range(4)]
+            )
         current = (residual_weight * state_wide + down_scale[layer_idx] * down_total).astype(
             jnp.bfloat16
         )

time: 363 us -> 401 us (1.10)
  waiting for transfers between devices: 241 us -> 277 us
  starting transfers between devices: 0.47 us -> 8.44 us
    ppermute x0 -> x4, waiting for transfers between devices: none -> 138 us  [on_device(): lax.ppermute(down_total, 'ra', [(dev, dev ^ hop) for dev in range(4)])]
    psum x2 -> x0, waiting for transfers between devices: 104 us -> none  [on_device(): down_total = lax.psum(partial_value, 'ra')]
    ppermute x0 -> x4, starting transfers between devices: none -> 8.04 us  [on_device(): lax.ppermute(down_total, 'ra', [(dev, dev ^ hop) for dev in range(4)])]
  transfers between devices with their start and end apart: 8 -> 10, of which waited for: 8 -> 10; matrix products, arithmetic and copies ran while one was open for 9% -> 8% of each run, Pallas kernels for 0% -> 0%
where the time goes in v1:
time: 401 us; the launch traced here: 400 us
  waiting for transfers between devices  277 us (69%)
  other arithmetic  39.6 us (10%)
  matrix products  30.9 us (8%)
  blocking collectives  20.5 us (5%)
  between operations  13.7 us (3%)
  local copies, waits for them, and re-layouts  10.5 us (3%)
  starting transfers between devices  8.44 us (2%)
    ppermute x4, waiting for transfers between devices, on_device(): lax.ppermute(down_total, 'ra', [(dev, dev ^ hop) for dev in range(4)])  138 us
    reduce_scatter x2, waiting for transfers between devices, on_device(): lax.psum_scatter(value_part, 'cb', scatter_dimension=1, tiled=True)  77.4 us
    reduce_scatter x2, waiting for transfers between devices, on_device(): lax.psum_scatter(gate_part, 'cb', scatter_dimension=1, tiled=True)  35.4 us
    another operation x3, other arithmetic  29.8 us
    all_gather x2, waiting for transfers between devices, on_device(): hidden = lax.all_gather(hidden, 'cb', axis=1, tiled=True)  25.4 us
    psum x3, blocking collectives, row_inverse(): lax.psum(jnp.sum(state_wide * state_wide, axis=1, keepdims=True), 'cb')  20.5 us
    dot_general x2, matrix products, on_device(): jnp.dot(scaled, gate_weight[layer_idx].astype(jnp.bfloat16), preferred_el...  10.7 us
    dot_general x2, matrix products, on_device(): jnp.dot(scaled, value_weight[layer_idx].astype(jnp.bfloat16), preferred_e...  10.6 us
  transfers between devices with their start and end apart: 10, of which 10 were waited for; matrix products, arithmetic and copies ran while one was open for 8% of the time, Pallas kernels for 0%

profile of v1, /device:TPU:0, one launch (start us, length us, event | category | flops | bytes accessed | tf_op | source)
XLA Modules:
  0.0 400.3 jit_solution(9945474060387361138)
XLA Ops:
  7.4 8.6 %convert.12 = bf16[2,1024,2816]{2,1,0:T(8,128)(2,1)S(1)} convert(f32[2,1024,2816]{2,1,0:T(8,128)} %param.12) | non-fusion elementwise | flops 5767168 | bytes 34603008 | tf_op jit(solution)/shard_map/convert.5
  16.0 4.2 %copy-done.1 = bf16[2,1024,2816]{2,1,0:T(8,128)(2,1)} copy-done((bf16[2,1024,2816]{2,1,0:T(8,128)(2,1)}, bf16[2,1024,2816]{2,1,0:T(8,128)(2,1)S(1)}, u32[]{:S(2)}) %copy-start.1) | copy-done | bytes 11534360
  20.2 4.1 %fusion.5 = f32[256,2816]{0,1:T(8,128)} fusion(bf16[2,1024,2816]{2,1,0:T(8,128)(2,1)S(1)} %convert.12, bf16[256,1024]{1,0:T(8,128)(2,1)S(1)} %copy-done.2, f32[1024]{0:T(1024)S(1)} %bitcast.42), kind=kOutput, calls=%fused_computation.11 | convolution fusion | flops 1477181440 | bytes 9179136 | tf_op jit(solution)/shard_map/dot_general | solution.py:44
  24.4 8.6 %convert.13 = bf16[2,1024,2816]{2,1,0:T(8,128)(2,1)S(1)} convert(f32[2,1024,2816]{2,1,0:T(8,128)} %param.13) | non-fusion elementwise | flops 5767168 | bytes 34603008 | tf_op jit(solution)/shard_map/convert.4
  33.0 4.8 %copy-done = bf16[2,1024,2816]{2,1,0:T(8,128)(2,1)} copy-done((bf16[2,1024,2816]{2,1,0:T(8,128)(2,1)}, bf16[2,1024,2816]{2,1,0:T(8,128)(2,1)S(1)}, u32[]{:S(2)}) %copy-start) | copy-done | bytes 11534360
  37.8 4.0 fusion.4
  42.2 9.0 %psum.21 = f32[256,1]{0,1:T(1,128)S(1)} all-reduce(f32[256,1]{0,1:T(1,128)S(1)} %bitcast.39), channel_id=1, replica_groups=mesh['grp'=2,'ra'=4,'cb'=4] {'cb'}, use_global_device_ids=true, to_apply=%region_1.0 | all-reduce | flops 256 | bytes 2048 | tf_op jit(solution)/shard_map/psum | solution.py:21
  51.5 12.1 %reduce-scatter.5.cloned.1.call-done = f32[256,704]{0,1:T(8,128)} async-done(((f32[256,2816]{0,1:T(8,128)}), f32[256,704]{0,1:T(8,128)}) %reduce-scatter.5.cloned.1.call-update) | async-done | bytes 720912 | tf_op jit(solution)/shard_map/reduce_scatter | solution.py:51
  63.5 38.8 %reduce-scatter.7.cloned.1.call-done = f32[256,704]{0,1:T(8,128)} async-done(((f32[256,2816]{0,1:T(8,128)}), f32[256,704]{0,1:T(8,128)}) %reduce-scatter.7.cloned.1.call-update) | async-done | bytes 720912 | tf_op jit(solution)/shard_map/reduce_scatter | solution.py:52
  106.2 12.6 %convert.14 = bf16[2,2816,1024]{2,1,0:T(8,128)(2,1)} convert(f32[2,2816,1024]{2,1,0:T(8,128)} %param.18) | non-fusion elementwise | flops 5767168 | bytes 34603008 | tf_op jit(solution)/shard_map/convert.3
  118.8 6.4 %all-gather.3.cloned.1.call-done = bf16[256,2816]{0,1:T(8,128)(2,1)} async-done(((bf16[256,704]{0,1:T(8,128)(2,1)}), bf16[256,2816]{0,1:T(8,128)(2,1)}) %all-gather.3.cloned.1.call-update) | async-done | bytes 1441808 | tf_op jit(solution)/shard_map/all_gather | solution.py:66
  125.2 4.8 %fusion.3 = f32[256,1024]{1,0:T(8,128)S(1)} fusion(bf16[256,2816]{0,1:T(8,128)(2,1)} %all-gather.3.cloned.1.call-done, bf16[2,2816,1024]{2,1,0:T(8,128)(2,1)} %convert.14), kind=kOutput, calls=%fused_computation.7 | convolution fusion | flops 1476395008 | bytes 8257536 | tf_op jit(solution)/shard_map/dot_general | solution.py:67
  131.5 23.8 %collective-permute-done = f32[256,1024]{1,0:T(8,128)S(1)} collective-permute-done((f32[256,1024]{1,0:T(8,128)S(1)}, f32[256,1024]{1,0:T(8,128)S(1)}, u32[]{:S(2)}, u32[]{:S(2)}) %collective-permute-start) | collective-permute-done | bytes 1048608 | tf_op jit(solution)/shard_map/ppermute | solution.py:72
  157.9 45.4 %collective-permute-done.1 = f32[256,1024]{1,0:T(8,128)S(1)} collective-permute-done((f32[256,1024]{1,0:T(8,128)S(1)}, f32[256,1024]{1,0:T(8,128)S(1)}, u32[]{:S(2)}, u32[]{:S(2)}) %collective-permute-start.1) | collective-permute-done | bytes 1048608 | tf_op jit(solution)/shard_map/ppermute | solution.py:72
  203.7 6.6 %fusion.2 = f32[256,2816]{0,1:T(8,128)} fusion(bf16[2,1024,2816]{2,1,0:T(8,128)(2,1)} %copy-done.1, bf16[256,1024]{1,0:T(8,128)(2,1)S(1)} %get-tuple-element.20, f32[1024]{0:T(1024)S(1)} %bitcast.40), kind=kOutput, calls=%fused_computation.5 | convolution fusion | flops 1477181440 | bytes 9179136 | tf_op jit(solution)/shard_map/dot_general | solution.py:44
  210.6 6.6 %fusion.1 = f32[256,2816]{0,1:T(8,128)} fusion(bf16[2,1024,2816]{2,1,0:T(8,128)(2,1)} %copy-done, bf16[256,1024]{1,0:T(8,128)(2,1)S(1)} %get-tuple-element.20, f32[1024]{0:T(1024)S(1)} %bitcast.41), kind=kOutput, calls=%fused_computation.3 | convolution fusion | flops 1477181440 | bytes 9179136 | tf_op jit(solution)/shard_map/dot_general | solution.py:47
  217.5 5.8 %psum.22 = f32[256,1]{0,1:T(1,128)S(1)} all-reduce(f32[256,1]{0,1:T(1,128)S(1)} %bitcast.34), channel_id=1, replica_groups=mesh['grp'=2,'ra'=4,'cb'=4] {'cb'}, use_global_device_ids=true, to_apply=%region_5.6 | all-reduce | flops 256 | bytes 2048 | tf_op jit(solution)/shard_map/psum | solution.py:21
  223.3 23.4 %reduce-scatter.9.cloned.1.call-done = f32[256,704]{0,1:T(8,128)} async-done(((f32[256,2816]{0,1:T(8,128)}), f32[256,704]{0,1:T(8,128)}) %reduce-scatter.9.cloned.1.call-update) | async-done | bytes 720912 | tf_op jit(solution)/shard_map/reduce_scatter | solution.py:51
  246.7 38.6 %reduce-scatter.11.cloned.1.call-done = f32[256,704]{0,1:T(8,128)} async-done(((f32[256,2816]{0,1:T(8,128)}), f32[256,704]{0,1:T(8,128)}) %reduce-scatter.11.cloned.1.call-update) | async-done | bytes 720912 | tf_op jit(solution)/shard_map/reduce_scatter | solution.py:52
  289.1 19.1 %all-gather.5.cloned.1.call-done = bf16[256,2816]{0,1:T(8,128)(2,1)} async-done(((bf16[256,704]{0,1:T(8,128)(2,1)}), bf16[256,2816]{0,1:T(8,128)(2,1)}) %all-gather.5.cloned.1.call-update) | async-done | bytes 1441808 | tf_op jit(solution)/shard_map/all_gather | solution.py:66
  308.1 4.8 %fusion = f32[256,1024]{1,0:T(8,128)S(1)} fusion(bf16[256,2816]{0,1:T(8,128)(2,1)} %all-gather.5.cloned.1.call-done, bf16[2,2816,1024]{2,1,0:T(8,128)(2,1)} %convert.14), kind=kOutput, calls=%fused_computation.1 | convolution fusion | flops 1476395008 | bytes 8257536 | tf_op jit(solution)/shard_map/dot_general | solution.py:67
  314.5 23.8 %collective-permute-done.2 = f32[256,1024]{1,0:T(8,128)S(1)} collective-permute-done((f32[256,1024]{1,0:T(8,128)S(1)}, f32[256,1024]{1,0:T(8,128)S(1)}, u32[]{:S(2)}, u32[]{:S(2)}) %collective-permute-start.2) | collective-permute-done | bytes 1048608 | tf_op jit(solution)/shard_map/ppermute | solution.py:72
  340.9 45.4 %collective-permute-done.3 = f32[256,1024]{1,0:T(8,128)S(1)} collective-permute-done((f32[256,1024]{1,0:T(8,128)S(1)}, f32[256,1024]{1,0:T(8,128)S(1)}, u32[]{:S(2)}, u32[]{:S(2)}) %collective-permute-start.3) | collective-permute-done | bytes 1048608 | tf_op jit(solution)/shard_map/ppermute | solution.py:72
  386.7 5.8 %psum.23 = f32[256,1]{0,1:T(1,128)S(1)} all-reduce(f32[256,1]{0,1:T(1,128)S(1)} %bitcast.37), channel_id=1, replica_groups=mesh['grp'=2,'ra'=4,'cb'=4] {'cb'}, use_global_device_ids=true, to_apply=%region_9.10 | all-reduce | flops 256 | bytes 2048 | tf_op jit(solution)/shard_map/psum | solution.py:21
  (53 shorter events, 19.8 us)
Async XLA Ops:
  6.5 57.0 %reduce-scatter.5.cloned.1.call-start = ((), (), s32[]{:S(2)}) async-start(), calls=%async_computation.4 | async-start | bytes 3604480 | tf_op jit(solution)/shard_map/reduce_scatter | solution.py:51
  7.4 12.8 %copy-start.2 = (bf16[256,1024]{1,0:T(8,128)(2,1)S(1)}, bf16[256,1024]{1,0:T(8,128)(2,1)}, u32[]{:S(2)}) copy-start(bf16[256,1024]{1,0:T(8,128)(2,1)} %param.10) | copy-start | bytes 1572868
  16.0 4.2 %copy-start.1 = (bf16[2,1024,2816]{2,1,0:T(8,128)(2,1)}, bf16[2,1024,2816]{2,1,0:T(8,128)(2,1)S(1)}, u32[]{:S(2)}) copy-start(bf16[2,1024,2816]{2,1,0:T(8,128)(2,1)S(1)} %convert.12) | copy-start | bytes 34603012
  24.3 78.0 %reduce-scatter.7.cloned.1.call-start = ((), (), s32[]{:S(2)}) async-start(), calls=%async_computation.5 | async-start | bytes 3604480 | tf_op jit(solution)/shard_map/reduce_scatter | solution.py:52
  32.9 4.8 %copy-start = (bf16[2,1024,2816]{2,1,0:T(8,128)(2,1)}, bf16[2,1024,2816]{2,1,0:T(8,128)(2,1)S(1)}, u32[]{:S(2)}) copy-start(bf16[2,1024,2816]{2,1,0:T(8,128)(2,1)S(1)} %convert.13) | copy-start | bytes 34603012
  37.7 4.1 %copy-start.5 = (f32[2,2816]{1,0:T(2,128)S(1)}, f32[2,2816]{1,0:T(2,128)}, u32[]{:S(2)}) copy-start(f32[2,2816]{1,0:T(2,128)} %param.14) | copy-start | bytes 67588
  37.8 4.1 %copy-start.6 = (f32[2,2816]{1,0:T(2,128)S(1)}, f32[2,2816]{1,0:T(2,128)}, u32[]{:S(2)}) copy-start(f32[2,2816]{1,0:T(2,128)} %param.15) | copy-start | bytes 67588
  37.8 13.5 %copy-start.3 = (f32[2,3,2816]{2,0,1:T(2,128)S(1)}, f32[2,3,2816]{2,0,1:T(2,128)}, u32[]{:S(2)}) copy-start(f32[2,3,2816]{2,0,1:T(2,128)} %param.16) | copy-start | bytes 202756
  37.8 13.5 %copy-start.4 = (f32[2,3,2816]{2,0,1:T(2,128)S(1)}, f32[2,3,2816]{2,0,1:T(2,128)}, u32[]{:S(2)}) copy-start(f32[2,3,2816]{2,0,1:T(2,128)} %param.17) | copy-start | bytes 202756
  41.8 83.4 %all-gather.3.cloned.1.call-start = ((), (), s32[]{:S(2)}) async-start(), calls=%async_computation.6 | async-start | bytes 1802240 | tf_op jit(solution)/shard_map/all_gather | solution.py:66
  106.1 140.5 %reduce-scatter.9.cloned.1.call-start = ((), (), s32[]{:S(2)}) async-start(), calls=%async_computation.7 | async-start | bytes 3604480 | tf_op jit(solution)/shard_map/reduce_scatter | solution.py:51
  118.8 39.2 %copy-start.7 = (f32[2,1024]{1,0:T(2,128)S(1)}, f32[2,1024]{1,0:T(2,128)}, u32[]{:S(2)}) copy-start(f32[2,1024]{1,0:T(2,128)} %param.19) | copy-start | bytes 24580
  129.9 25.4 %collective-permute-start = (f32[256,1024]{1,0:T(8,128)S(1)}, f32[256,1024]{1,0:T(8,128)S(1)}, u32[]{:S(2)}, u32[]{:S(2)}) collective-permute-start(f32[256,1024]{1,0:T(8,128)S(1)} %fusion.3), channel_id=1, source_target_pairs={{0,4},{4,0},{8,12},{12,8},{1,5},{5,1},{9,13},{13,9},{2,6},{6,2},{1... | collective-permute-start | bytes 3145736 | tf_op jit(solution)/shard_map/ppermute | solution.py:72
  155.5 47.9 %collective-permute-start.1 = (f32[256,1024]{1,0:T(8,128)S(1)}, f32[256,1024]{1,0:T(8,128)S(1)}, u32[]{:S(2)}, u32[]{:S(2)}) collective-permute-start(f32[256,1024]{1,0:T(8,128)S(1)} %add.103), channel_id=1, source_target_pairs={{0,8},{4,12},{8,0},{12,4},{1,9},{5,13},{9,1},{13,5},{2,10},{6,14},... | collective-permute-start | bytes 3145736 | tf_op jit(solution)/shard_map/ppermute | solution.py:72
  210.3 75.0 %reduce-scatter.11.cloned.1.call-start = ((), (), s32[]{:S(2)}) async-start(), calls=%async_computation.8 | async-start | bytes 3604480 | tf_op jit(solution)/shard_map/reduce_scatter | solution.py:52
  217.2 90.9 %all-gather.5.cloned.1.call-start = ((), (), s32[]{:S(2)}) async-start(), calls=%async_computation.9 | async-start | bytes 1802240 | tf_op jit(solution)/shard_map/all_gather | solution.py:66
  312.9 25.4 %collective-permute-start.2 = (f32[256,1024]{1,0:T(8,128)S(1)}, f32[256,1024]{1,0:T(8,128)S(1)}, u32[]{:S(2)}, u32[]{:S(2)}) collective-permute-start(f32[256,1024]{1,0:T(8,128)S(1)} %fusion), channel_id=1, source_target_pairs={{0,4},{4,0},{8,12},{12,8},{1,5},{5,1},{9,13},{13,9},{2,6},{6,2},{1... | collective-permute-start | bytes 3145736 | tf_op jit(solution)/shard_map/ppermute | solution.py:72
  338.4 47.9 %collective-permute-start.3 = (f32[256,1024]{1,0:T(8,128)S(1)}, f32[256,1024]{1,0:T(8,128)S(1)}, u32[]{:S(2)}, u32[]{:S(2)}) collective-permute-start(f32[256,1024]{1,0:T(8,128)S(1)} %add.113), channel_id=1, source_target_pairs={{0,8},{4,12},{8,0},{12,4},{1,9},{5,13},{9,1},{13,5},{2,10},{6,14},... | collective-permute-start | bytes 3145736 | tf_op jit(solution)/shard_map/ppermute | solution.py:72
Sparse Core Ops, SparseCore 0:
  24.4 39.0 reduce-scatter.4
  66.1 36.1 reduce-scatter.6
  106.2 18.8 all-gather.2
  210.4 36.1 reduce-scatter.8
  249.0 36.1 reduce-scatter.10
  289.2 18.8 all-gather.4
